TPU v7x, 32 devices: a whole 2x2x4 slice. The times are simulated.
32 devices in a mesh: sp: 8 (over z, y), tp: 4 (over x, core).
Axes of the slice: x: 2, y: 2, z: 4, core: 2. Of those that a mesh axis runs over, the one named last changes fastest.
Arguments:
- b_gate: bfloat16 [4096, 2048], P('sp', 'tp'), may hold values from -6 to 6
- c_gate: bfloat16 [4096, 2048], P('sp', 'tp'), may hold values from -6 to 6
- values_in: bfloat16 [4096, 2048], P('sp', 'tp'), may hold values from -6 to 6
- conv_taps: float32 [3, 2048], P(None, 'tp'), may hold values from -4 to 4
- out_proj: bfloat16 [2048, 2048], P('tp'), may hold values from -0.125 to 0.125
- resid: bfloat16 [4096, 2048], P(('sp', 'tp')), may hold values from -6 to 6
- post_gain: float32 [2048], replicated, may hold values from 0.1 to 1.9
- pre_gain: float32 [2048], replicated, may hold values from 0.1 to 1.9
- moe_gain: float32 [2048], replicated, may hold values from 0.1 to 1.9
- routes: int32 [4096, 4], P(('sp', 'tp')), may hold values from 0 to 7, all different within a row; in each aligned block of 128 rows (0 to 127, 128 to 255, ...) at most 128 rows name the same one
- route_weight: float32 [4096, 4], P(('sp', 'tp')), may hold values from 0.1 to 1
- gate_w: bfloat16 [8, 2048, 640], P('sp'), may hold values from -1 to 1
- up_w: bfloat16 [8, 2048, 640], P('sp'), may hold values from -1 to 1
- down_w: bfloat16 [8, 640, 2048], P('sp'), may hold values from -0.25 to 0.25
Outputs:
- result: bfloat16 [4096, 2048], P(('sp', 'tp'))
Inputs may be any that keep to these rules, and one draw needn't show every extreme that they name: `routes`: each row names 4 different experts; within each aligned block of 128 rows no expert is named by more than 128 rows.
All inputs are finite; a program needn't handle non-finite values.
Results may differ from a plain program's by a relative error of at most 0.007.
Values may be sent and summed in bfloat16 or wider, within the bound.
A program may use at most 64 MiB of HBM per device.

v0:
```python
import functools

import jax
import jax.numpy as jnp
from jax import lax
from jax.experimental import pallas as pl
from jax.experimental.pallas import tpu as pltpu
from jax.sharding import PartitionSpec as P

epsilon = 1e-06


def shifted(shard, axis, by):
    devices = lax.axis_size(axis)
    pairs = [(i, i + by) for i in range(devices) if 0 <= i + by < devices]
    return lax.ppermute(shard, axis, pairs)


def rms_norm(vector, gain):
    return vector * lax.rsqrt(jnp.mean(vector * vector, axis=-1, keepdims=True) + epsilon) * gain


def expert_rows(rows_in, gate_w, up_w, down_w):
    gate_pre = jnp.dot(rows_in, gate_w[0], preferred_element_type=jnp.float32)
    up_pre = jnp.dot(rows_in, up_w[0], preferred_element_type=jnp.float32)
    gate_act = jnp.minimum(gate_pre, 7.0)
    up_act = jnp.clip(up_pre, -7.0, 7.0)
    hidden = (gate_act * jax.nn.sigmoid(1.702 * gate_act) * (up_act + 1.0)).astype(jnp.bfloat16)
    return jnp.dot(hidden, down_w[0], preferred_element_type=jnp.float32).astype(jnp.bfloat16)


def by_slot(normed, routes, route_weight, gate_w, up_w, down_w):
    own_count = normed.shape[0]
    width = normed.shape[1]
    top_count = routes.shape[1]
    experts = lax.axis_size("sp")
    capacity = 2 * own_count * top_count // experts
    flat_ids = routes.reshape(-1)
    assigned = flat_ids.shape[0]
    onehot = (flat_ids[:, None] == jnp.arange(experts, dtype=jnp.int32)[None, :]).astype(jnp.int32)
    earlier = jnp.cumsum(onehot, axis=0) - onehot
    slot_index = jnp.sum(earlier * onehot, axis=1)
    target = flat_ids * capacity + slot_index
    source = (
        jnp.full((experts * capacity,), assigned, jnp.int32)
        .at[target]
        .set(jnp.arange(assigned, dtype=jnp.int32))
    )
    row_index = jnp.where(source < assigned, source // top_count, own_count)
    with_blank = jnp.concatenate([normed, jnp.zeros((1, width), jnp.bfloat16)], axis=0)
    outgoing = with_blank[row_index].reshape(experts, capacity, width)
    slots_in = lax.all_to_all(outgoing, "sp", split_axis=0, concat_axis=0, tiled=True)
    expert_out = expert_rows(slots_in, gate_w, up_w, down_w)
    returned = lax.all_to_all(expert_out, "sp", split_axis=0, concat_axis=0, tiled=True)
    chosen = returned.reshape(experts * capacity, width)[target].astype(jnp.float32)
    weighted = chosen * route_weight.reshape(-1)[:, None]
    combined = jnp.sum(weighted.reshape(own_count, top_count, width), axis=1)
    return combined


def copy_to(axis, device, src, dst, send_sem, recv_sem):
    return pltpu.make_async_remote_copy(
        src_ref=src,
        dst_ref=dst,
        send_sem=send_sem,
        recv_sem=recv_sem,
        device_id={axis: device},
        device_id_type=pl.DeviceIdType.MESH,
    )


def greet_all(axis, n):
    me = lax.axis_index(axis)
    barrier = pltpu.get_barrier_semaphore()
    for step in range(1, n):
        pl.semaphore_signal(
            barrier,
            inc=1,
            device_id={axis: lax.rem(me + step, n)},
            device_id_type=pl.DeviceIdType.MESH,
        )
    pl.semaphore_wait(barrier, n - 1)


def on_line(place, length):
    return jnp.logical_and(place >= 0, place < length)


def gather_kernel(axis, n, early, own, spread, out, weights, *sems):
    own_sem, pair_s, pair_r, line_s, line_r, both_s, both_r, w_s, w_r = sems
    length = n // 2
    me = lax.axis_index(axis)
    place, side = me // 2, lax.rem(me, 2)
    mate = place * 2 + 1 - side
    rows = own.shape[0]
    head, tail = pl.ds(0, early), pl.ds(early, rows - early)
    greet_all(axis, n)

    def pair_copy(origin, k, part, src=None):
        slot = out.at[origin * 2 + side, part]
        return copy_to(axis, mate, slot if src is None else src, slot, pair_s.at[k], pair_r.at[k])

    def line_copy(origin, way, k, sem, src=None):
        slot = out.at[origin * 2 + side, tail]
        return copy_to(
            axis,
            lax.rem(place + way + length, length) * 2 + side,
            slot if src is None else src,
            slot,
            line_s.at[k, sem],
            line_r.at[k, sem],
        )

    def both_copy(origin, member, way, k, sem):
        slot = out.at[origin * 2 + member, head]
        return copy_to(
            axis,
            lax.rem(place + way + length, length) * 2 + side,
            slot,
            slot,
            both_s.at[k, sem, member],
            both_r.at[k, sem, member],
        )

    ways = ((1, 0), (-1, 1))
    here = pltpu.make_async_copy(own, out.at[me], own_sem)
    here.start()
    swap = pair_copy(place, 2 * length, head, own.at[head])
    swap.start()
    for way, sem in ways:
        @pl.when(on_line(place + way, length))
        def _():
            line_copy(place, way, 0, sem, own.at[tail]).start()
    pair_copy(place, 0, tail, own.at[tail]).start()
    for step in range(1, n):
        expert = lax.rem(me + step, n)
        copy_to(axis, expert, spread.at[expert], weights.at[me], w_s.at[step], w_r.at[step]).start()
    weights[me] = spread[me]
    here.wait()
    swap.wait_recv()
    for way, sem in ways:
        @pl.when(on_line(place + way, length))
        def _():
            for member in range(2):
                both_copy(place, member, way, 0, sem).start()
    for k in range(1, length):
        for way, sem in ways:
            origin = place - way * k
            @pl.when(on_line(origin, length))
            def _():
                line_copy(origin, way, k - 1, sem).wait_recv()

                @pl.when(on_line(place + way, length))
                def _():
                    line_copy(origin, way, k, sem).start()
                pair_copy(origin, 2 * k - sem, tail).start()
        for way, sem in ways:
            origin = place - way * k
            @pl.when(on_line(origin, length))
            def _():
                for member in range(2):
                    both_copy(origin, member, way, k - 1, sem).wait_recv()

                    @pl.when(on_line(place + way, length))
                    def _():
                        both_copy(origin, member, way, k, sem).start()
    swap.wait_send()
    pair_copy(place, 0, tail).wait()
    for step in range(1, n):
        expert = lax.rem(me + step, n)
        copy_to(axis, expert, spread.at[expert], weights.at[me], w_s.at[step], w_r.at[step]).wait()
    for k in range(length):
        for way, sem in ways:
            origin = place - way * k
            @pl.when(on_line(origin, length))
            def _():
                if k > 0:
                    pair_copy(origin, 2 * k - sem, tail).wait()

                @pl.when(on_line(place + way, length))
                def _():
                    line_copy(origin, way, k, sem).wait_send()
                    for member in range(2):
                        both_copy(origin, member, way, k, sem).wait_send()


def gather_rows(axis, own, spread, collective_id):
    n = lax.axis_size(axis)
    rows, width = own.shape
    length = n // 2
    early = rows * 3 // 8 // 16 * 16
    vmem = pl.BlockSpec(memory_space=pltpu.VMEM)
    dma = pltpu.SemaphoreType.DMA
    return pl.pallas_call(
        functools.partial(gather_kernel, axis, n, early),
        out_shape=(
            jax.ShapeDtypeStruct((n, rows, width), own.dtype),
            jax.ShapeDtypeStruct((n, 1, rows), spread.dtype),
        ),
        in_specs=[vmem, vmem],
        out_specs=(vmem, vmem),
        scratch_shapes=[
            dma,
            dma((2 * length + 1,)),
            dma((2 * length + 1,)),
            dma((length, 2)),
            dma((length, 2)),
            dma((length, 2, 2)),
            dma((length, 2, 2)),
            dma((n,)),
            dma((n,)),
        ],
        compiler_params=pltpu.CompilerParams(collective_id=collective_id, has_side_effects=True),
    )(own, spread)


def reduce_kernel(axis, n, early, part, out, *scratch):
    pair_in, line_in, line_out, swap_in, swap_out, both_in, both_out = scratch[:7]
    pair_s, pair_r, line_s, line_r, both_s, both_r, swap_s, swap_r = scratch[7:]
    length = n // 2
    me = lax.axis_index(axis)
    place, side = me // 2, lax.rem(me, 2)
    mate = place * 2 + 1 - side
    rows = part.shape[1]
    head, tail = pl.ds(0, early), pl.ds(early, rows - early)
    ways = ((1, 0), (-1, 1))
    f32 = jnp.float32
    greet_all(axis, n)

    def pair_copy(target, k):
        return copy_to(
            axis, mate, part.at[target * 2 + 1 - side, tail], pair_in.at[k], pair_s.at[k], pair_r.at[k]
        )

    def line_copy(way, k, sem):
        return copy_to(
            axis,
            lax.rem(place + way + length, length) * 2 + side,
            line_out.at[k, sem],
            line_in.at[k - 1, sem],
            line_s.at[k, sem],
            line_r.at[k - 1, sem],
        )

    def line_arrival(way, k, sem):
        return copy_to(
            axis,
            lax.rem(place - way + length, length) * 2 + side,
            line_out.at[k, sem],
            line_in.at[k, sem],
            line_s.at[k, sem],
            line_r.at[k, sem],
        )

    def both_copy(way, k, sem, member):
        return copy_to(
            axis,
            lax.rem(place + way + length, length) * 2 + side,
            both_out.at[k, sem, member],
            both_in.at[k - 1, sem, member],
            both_s.at[k, sem, member],
            both_r.at[k - 1, sem, member],
        )

    def both_arrival(way, k, sem, member):
        return copy_to(
            axis,
            lax.rem(place - way + length, length) * 2 + side,
            both_out.at[k, sem, member],
            both_in.at[k, sem, member],
            both_s.at[k, sem, member],
            both_r.at[k, sem, member],
        )

    def slot_of(k, sem):
        return 2 * k - sem if k else 0

    for k in range(length - 1, -1, -1):
        for way, sem in ways[: 2 if k else 1]:
            target = place + way * k
            @pl.when(on_line(target, length))
            def _():
                pair_copy(target, slot_of(k, sem)).start()
    for k in range(length - 1, 0, -1):
        for way, sem in ways if early else ():
            target = place + way * k
            @pl.when(on_line(target, length))
            def _():
                for member in range(2):
                    both_out[k, sem, member] = part[target * 2 + member, head]

                    @pl.when(on_line(place - way, length))
                    def _():
                        both_arrival(way, k, sem, member).wait_recv()
                        total = part[target * 2 + member, head].astype(f32)
                        total = total + both_in[k, sem, member].astype(f32)
                        both_out[k, sem, member] = total.astype(part.dtype)
                    both_copy(way, k, sem, member).start()
        for way, sem in ways:
            target = place + way * k
            @pl.when(on_line(target, length))
            def _():
                slot = slot_of(k, sem)
                pair_copy(target, slot).wait_recv()
                total = part[target * 2 + side, tail].astype(f32) + pair_in[slot].astype(f32)

                @pl.when(jnp.logical_not(on_line(place - way, length)))
                def _():
                    line_out[k, sem] = total.astype(part.dtype)

                @pl.when(on_line(place - way, length))
                def _():
                    line_arrival(way, k, sem).wait_recv()
                    more = total + line_in[k, sem].astype(f32)
                    line_out[k, sem] = more.astype(part.dtype)
                line_copy(way, k, sem).start()
    if early:
        for member in range(2):
            swap_out[member] = part[place * 2 + member, head].astype(f32)
            for way, sem in ways:
                @pl.when(on_line(place - way, length))
                def _():
                    both_arrival(way, 0, sem, member).wait_recv()
                    swap_out[member] += both_in[0, sem, member].astype(f32)
        swap_in[0] = swap_out[1 - side].astype(part.dtype)
        swap = copy_to(axis, mate, swap_in.at[0], swap_in.at[1], swap_s, swap_r)
        swap.start()
    pair_copy(place, 0).wait_recv()
    out[tail] = part[place * 2 + side, tail].astype(f32) + pair_in[0].astype(f32)
    for way, sem in ways:
        @pl.when(on_line(place - way, length))
        def _():
            line_arrival(way, 0, sem).wait_recv()
            out[tail] += line_in[0, sem].astype(f32)
    if early:
        swap.wait()
        out[head] = swap_out[side] + swap_in[1].astype(f32)
    for k in range(length - 1, -1, -1):
        for way, sem in ways[: 2 if k else 1]:
            target = place + way * k
            @pl.when(on_line(target, length))
            def _():
                pair_copy(target, slot_of(k, sem)).wait_send()
                if k:
                    line_copy(way, k, sem).wait_send()
                    if early:
                        for member in range(2):
                            both_copy(way, k, sem, member).wait_send()


def reduce_rows(axis, part, early, collective_id):
    n, rows, width = part.shape
    length = n // 2
    late = rows - early
    vmem = pl.BlockSpec(memory_space=pltpu.VMEM)
    dma = pltpu.SemaphoreType.DMA
    first = max(early, 16)
    return pl.pallas_call(
        functools.partial(reduce_kernel, axis, n, early),
        out_shape=jax.ShapeDtypeStruct((rows, width), jnp.float32),
        in_specs=[vmem],
        out_specs=vmem,
        scratch_shapes=[
            pltpu.VMEM((2 * length, late, width), part.dtype),
            pltpu.VMEM((length, 2, late, width), part.dtype),
            pltpu.VMEM((length, 2, late, width), part.dtype),
            pltpu.VMEM((2, first, width), part.dtype),
            pltpu.VMEM((2, first, width), jnp.float32),
            pltpu.VMEM((length, 2, 2, first, width), part.dtype),
            pltpu.VMEM((length, 2, 2, first, width), part.dtype),
            dma((2 * length,)),
            dma((2 * length,)),
            dma((length, 2)),
            dma((length, 2)),
            dma((length, 2, 2)),
            dma((length, 2, 2)),
            dma,
            dma,
        ],
        compiler_params=pltpu.CompilerParams(collective_id=collective_id, has_side_effects=True),
    )(part)


def every_row(normed, routes, route_weight, gate_w, up_w, down_w):
    experts = lax.axis_size("sp")
    rows, width = normed.shape
    named = routes[:, :, None] == jnp.arange(experts, dtype=jnp.int32)[None, None, :]
    spread = jnp.sum(jnp.where(named, route_weight[:, :, None], 0.0), axis=1)
    gathered, weights = gather_rows("sp", normed, spread.T[:, None, :], 1)
    rows_in = gathered.reshape(experts * rows, width)
    expert_out = expert_rows(rows_in, gate_w, up_w, down_w)
    weighted = expert_out.astype(jnp.float32) * weights.reshape(experts * rows)[:, None]
    part = weighted.astype(jnp.bfloat16).reshape(experts, rows, width)
    return reduce_rows("sp", part, rows * 3 // 8 // 16 * 16, 2)


def body(
    b_gate,
    c_gate,
    values_in,
    conv_taps,
    out_proj,
    resid,
    post_gain,
    pre_gain,
    moe_gain,
    routes,
    route_weight,
    gate_w,
    up_w,
    down_w,
):
    tok_rows = b_gate.shape[0]
    product = c_gate.astype(jnp.float32) * values_in.astype(jnp.float32)
    prior_rows = shifted(product[tok_rows - 2 :], "sp", 1)
    padded = jnp.concatenate([prior_rows, product], axis=0)
    filtered = (
        padded[0:tok_rows] * conv_taps[0]
        + padded[1 : tok_rows + 1] * conv_taps[1]
        + padded[2 : tok_rows + 2] * conv_taps[2]
    )
    mixed_rows = (b_gate.astype(jnp.float32) * filtered).astype(jnp.bfloat16)
    experts = lax.axis_size("sp")
    own_count = resid.shape[0]
    whole_rows = 2 * own_count * routes.shape[1] // experts >= own_count
    share = jnp.dot(mixed_rows, out_proj, preferred_element_type=jnp.float32)
    if whole_rows:
        blocks = share.astype(jnp.bfloat16).reshape(-1, own_count, share.shape[1])
        projected = reduce_rows("tp", blocks, 0, 3)
    else:
        projected = lax.psum_scatter(share, "tp", scatter_dimension=0, tiled=True)
    stream = (resid.astype(jnp.float32) + rms_norm(projected, post_gain)).astype(jnp.bfloat16)
    normed = rms_norm(stream.astype(jnp.float32), pre_gain).astype(jnp.bfloat16)
    mix = every_row if whole_rows else by_slot
    combined = mix(normed, routes, route_weight, gate_w, up_w, down_w)
    return (stream.astype(jnp.float32) + rms_norm(combined, moe_gain)).astype(jnp.bfloat16)


def solution(mesh):
    placed = (
        P("sp", "tp"),
        P("sp", "tp"),
        P("sp", "tp"),
        P(None, "tp"),
        P("tp", None),
        P(("sp", "tp"), None),
        P(),
        P(),
        P(),
        P(("sp", "tp"), None),
        P(("sp", "tp"), None),
        P("sp", None, None),
        P("sp", None, None),
        P("sp", None, None),
    )
    return jax.shard_map(
        body, mesh=mesh, in_specs=placed, out_specs=P(("sp", "tp"), None), check_vma=False
    )
```

profile of v0, /device:TPU:8, one launch (start us, length us, event | category | flops | bytes accessed | tf_op | source)
XLA Modules:
  0.0 167.8 jit_solution(11800457956906576880)
XLA Ops:
  0.0 0.0 copy-start
  0.0 1.5 convert_multiply_fusion.2
  1.5 3.4 %collective-permute-start = (f32[2,512]{1,0:T(2,128)S(1)}, f32[2,512]{1,0:T(2,128)S(1)}, u32[]{:S(2)}, u32[]{:S(2)}) collective-permute-start(f32[2,512]{1,0:T(2,128)S(1)} %slice.24), channel_id=1, source_target_pairs={{0,4},{4,8},{8,12},{12,16},{16,20},{20,24},{24,28},{1,5},{5,9},{9,... | collective-permute-start | bytes 12296 | tf_op jit(solution)/shard_map/ppermute | solution.py:16
  5.0 0.8 fusion.29
  5.8 1.3 select_reduce_fusion
  7.1 0.8 collective-permute-done
  7.9 4.5 %convolution_convert_fusion = bf16[512,2048]{1,0:T(8,128)(2,1)} fusion(bf16[512,2048]{1,0:T(8,128)(2,1)} %param.18, f32[2,512]{1,0:T(2,128)S(1)} %collective-permute-done, f32[512,512]{1,0:T(8,128)S(1)} %convert_multiply_fusion.2, bf16[512,512]{1,0:T(8,128)(2,1)} %param.14, f32[512]{0:T(512)S(1)} %bitcast.30, f32[512]{0:T(512)S(1)} %bitcast.31, ...), kind=kOutput, calls=%fused_computation.1 | convolution fusion | flops 1077411840 | bytes 5777408 | tf_op jit(solution)/shard_map/dot_general | solution.py:426
  12.4 0.0 copy-start.1
  12.5 0.0 copy-start.2
  12.5 19.2 %shard_map.136 = f32[128,2048]{1,0:T(8,128)} custom-call(bf16[4,128,2048]{2,1,0:T(8,128)(2,1)} %bitcast.27), custom_call_target="tpu_custom_call" | custom-call | tf_op jit(solution)/shard_map/pallas_call | solution.py:358
  31.7 1.4 multiply_reduce_fusion.1
  33.1 0.0 copy-done.1
  33.1 1.7 %fusion.13 = (f32[128]{0:T(128)S(1)}, bf16[128,2048]{1,0:T(8,128)(2,1)S(1)}) fusion(f32[2048]{0:T(1024)S(1)} %copy-done.1, f32[128,2048]{1,0:T(8,128)} %shard_map.136, f32[128]{0:T(128)S(1)} %add_rsqrt_fusion.2, bf16[128,2048]{1,0:T(8,128)(2,1)} %param.19), kind=kLoop, calls=%fused_computation.19 | loop fusion | flops 2097024 | bytes 2106368 | tf_op jit(solution)/shard_map/reduce_sum | solution.py:20
  34.8 0.0 copy-done.2
  34.8 1.0 fusion.15.own
  35.8 52.8 %shard_map.137 = (bf16[8,128,2048]{2,1,0:T(8,128)(2,1)}, f32[8,1,128]{2,1,0:T(1,128)}) custom-call(bf16[128,2048]{1,0:T(8,128)(2,1)} %fusion.15.own, f32[8,1,128]{2,1,0:T(1,128)} %bitcast.28), custom_call_target="tpu_custom_call" | custom-call | tf_op jit(solution)/shard_map/pallas_call | solution.py:194
  88.6 0.0 copy-start.4
  88.6 8.0 %fusion.1 = f32[1024,640]{1,0:T(8,128)} fusion(bf16[1024,2048]{1,0:T(8,128)(2,1)} %bitcast.32, bf16[1,2048,640]{2,1,0:T(8,128)(2,1)} %param.26), kind=kOutput, calls=%fused_computation.3 | convolution fusion | flops 2684354560 | bytes 9437184 | tf_op jit(solution)/shard_map/dot_general | solution.py:25
  96.6 0.0 copy-done
  96.6 0.0 copy-done.4
  96.6 12.2 %multiply_convert_fusion = bf16[1024,2048]{1,0:T(8,128)(2,1)} fusion(f32[1024]{0:T(1024)S(1)} %bitcast.34, bf16[1,640,2048]{2,1,0:T(8,128)(2,1)S(1)} %copy-done, f32[1024,640]{1,0:T(8,128)} %fusion.1, bf16[1024,2048]{1,0:T(8,128)(2,1)} %bitcast.33, bf16[1,2048,640]{2,1,0:T(8,128)(2,1)} %param.25), kind=kOutput, calls=%fused_computation | convolution fusion | flops 5383651328 | bytes 16257024 | tf_op jit(solution)/shard_map/dot_general | solution.py:29
  108.8 0.0 copy-start.3
  108.8 55.4 %shard_map.138 = f32[128,2048]{1,0:T(8,128)} custom-call(bf16[8,128,2048]{2,1,0:T(8,128)(2,1)} %bitcast.26), custom_call_target="tpu_custom_call" | custom-call | tf_op jit(solution)/shard_map/pallas_call | solution.py:358
  164.2 1.4 multiply_reduce_fusion
  165.5 0.0 copy-done.3
  165.5 2.2 %fusion.16 = bf16[128,2048]{1,0:T(8,128)(2,1)} fusion(bf16[128,2048]{1,0:T(8,128)(2,1)S(1)} %get-tuple-element.10, f32[128,2048]{1,0:T(8,128)} %shard_map.138, f32[2048]{0:T(1024)S(1)} %copy-done.3, f32[128]{0:T(128)S(1)} %add_rsqrt_fusion), kind=kLoop, calls=%fused_computation.22 | loop fusion | flops 1310720 | bytes 2105856 | tf_op jit(solution)/shard_map/convert_element_type | solution.py:436
  (4 shorter events, 0.0 us)
Async XLA Ops:
  0.0 96.6 %copy-start = (bf16[1,640,2048]{2,1,0:T(8,128)(2,1)S(1)}, bf16[1,640,2048]{2,1,0:T(8,128)(2,1)}, u32[]{:S(2)}) copy-start(bf16[1,640,2048]{2,1,0:T(8,128)(2,1)} %param.27) | copy-start | bytes 7864324
  1.5 6.4 %collective-permute-start = (f32[2,512]{1,0:T(2,128)S(1)}, f32[2,512]{1,0:T(2,128)S(1)}, u32[]{:S(2)}, u32[]{:S(2)}) collective-permute-start(f32[2,512]{1,0:T(2,128)S(1)} %slice.24), channel_id=1, source_target_pairs={{0,4},{4,8},{8,12},{12,16},{16,20},{20,24},{24,28},{1,5},{5,9},{9,... | collective-permute-start | bytes 12296 | tf_op jit(solution)/shard_map/ppermute | solution.py:16
  12.4 20.6 %copy-start.1 = (f32[2048]{0:T(1024)S(1)}, f32[2048]{0:T(1024)}, u32[]{:S(2)}) copy-start(f32[2048]{0:T(1024)} %param.20) | copy-start | bytes 24580
  12.5 22.4 %copy-start.2 = (f32[2048]{0:T(1024)S(1)}, f32[2048]{0:T(1024)}, u32[]{:S(2)}) copy-start(f32[2048]{0:T(1024)} %param.21) | copy-start | bytes 24580
  88.6 8.0 %copy-start.4 = (f32[8,1,128]{2,1,0:T(1,128)S(1)}, f32[8,1,128]{2,1,0:T(1,128)}, u32[]{:S(2)}) copy-start(f32[8,1,128]{2,1,0:T(1,128)} %get-tuple-element.8) | copy-start | bytes 12292
  108.8 56.8 %copy-start.3 = (f32[2048]{0:T(1024)S(1)}, f32[2048]{0:T(1024)}, u32[]{:S(2)}) copy-start(f32[2048]{0:T(1024)} %param.22) | copy-start | bytes 24580
where the time goes:
time: 168 us
  Pallas kernels  127 us (76%)
  matrix products  24.7 us (15%)
  other arithmetic  10.5 us (6%)
  starting transfers between devices  3.43 us (2%)
    pallas_call x2, Pallas kernels, reduce_rows(): pl.pallas_call(functools.partial(reduce_kernel, axis, n, early), out_shap...  74.6 us
    pallas_call x1, Pallas kernels, gather_rows(): pl.pallas_call(functools.partial(gather_kernel, axis, n, early), out_shap...  52.8 us
    dot_general x1, matrix products, expert_rows(): jnp.dot(hidden, down_w[0], preferred_element_type=jnp.float32)  12.2 us
    dot_general x1, matrix products, expert_rows(): up_pre = jnp.dot(rows_in, up_w[0], preferred_element_type=jnp.float32)  8.01 us
    dot_general x1, matrix products, body(): share = jnp.dot(mixed_rows, out_proj, preferred_element_type=jnp.float32)  4.53 us
    reduce_sum x3, other arithmetic, rms_norm(): jnp.mean(vector * vector, axis=-1, keepdims=True) + epsilon  4.49 us
    ppermute x1, starting transfers between devices, shifted(): return lax.ppermute(shard, axis, pairs)  3.43 us
  transfers between devices with their start and end apart: 1, of which 1 were waited for; matrix products, arithmetic and copies ran while one was open for 1% of the time, Pallas kernels for 0%

commit v1 on v0

--- a/solution.py
+++ b/solution.py
@@ -392,6 +392,353 @@
     weighted = expert_out.astype(jnp.float32) * weights.reshape(experts * rows)[:, None]
     part = weighted.astype(jnp.bfloat16).reshape(experts, rows, width)
     return reduce_rows("sp", part, rows * 3 // 8 // 16 * 16, 2)
+
+
+def expert_kernel(n, t_n, cross, own, spread, gate, up, down, out, *scratch):
+    x_buf, w_in, w_out, hid, hid_out, part, red_in, red_out, w_row, w_col = scratch[:10]
+    (load_s, w_s, w_r, zt_s, zt_r, zh_s, zh_r, yt_s, yt_r, yh_s, yh_r,
+     h_s, h_r, red_s, red_r, dy_s, dy_r, dt_s, dt_r, dm_s, dm_r) = scratch[10:]
+    length = n // 2
+    f32, bf16 = jnp.float32, jnp.bfloat16
+    me = lax.axis_index("sp")
+    p, side = me // 2, lax.rem(me, 2)
+    mate = p * 2 + 1 - side
+    rows, width = own.shape
+    half = rows // 2
+    keep = half - cross
+    hidden = gate.shape[2]
+    lanes = 128
+    tiles = hidden // lanes
+    t_me = lax.axis_index("tp")
+    core = lax.rem(t_me, 2)
+    t_mate = t_me + 1 - 2 * core
+    share = hidden // t_n
+    last = length - 1
+    ways = ((0, 1), (1, -1))
+
+    loads = []
+    for j in range(tiles):
+        for m, src in enumerate((gate, up)):
+            loads.append(pltpu.make_async_copy(
+                src.at[0, :, pl.ds(j * lanes, lanes)],
+                w_in.at[:, pl.ds((2 * j + m) * lanes, lanes)],
+                load_s.at[2 * j + m]))
+    loads.append(pltpu.make_async_copy(down.at[0], w_out.at[pl.ds(0, hidden)], load_s.at[2 * tiles]))
+    for load in loads:
+        load.start()
+    place_own = pltpu.make_async_copy(own, x_buf.at[p, side], load_s.at[2 * tiles + 1])
+    place_own.start()
+    barrier = pltpu.get_barrier_semaphore()
+    for axis, count in (("sp", n), ("tp", t_n)):
+        here = lax.axis_index(axis)
+        for step in range(1, count):
+            pl.semaphore_signal(
+                barrier,
+                inc=1,
+                device_id={axis: lax.rem(here + step, count)},
+                device_id_type=pl.DeviceIdType.MESH,
+            )
+    pl.semaphore_wait(barrier, n + t_n - 2)
+
+    def down_slot(t):
+        return w_out.at[pl.ds(hidden + t * share, share)]
+
+    down_y = copy_to("sp", mate, down.at[0, pl.ds(t_me * share, share)], down_slot(t_me), dy_s, dy_r)
+
+    def down_x(step):
+        there = lax.rem(t_me + 2 * step, t_n)
+        return copy_to("tp", there, down_slot(t_me), down_slot(t_me), dt_s.at[step], dt_r.at[step])
+
+    def down_mate(step):
+        origin = lax.rem(t_me + t_n - 2 * step, t_n)
+        return copy_to("tp", t_mate, down_slot(origin), down_slot(origin), dm_s.at[step], dm_r.at[step])
+
+    def weight_copy(step):
+        expert = lax.rem(me + step, n)
+        return copy_to("sp", expert, spread.at[expert], w_row.at[me], w_s.at[step], w_r.at[step])
+
+    def at_rows(c, first, count):
+        return pl.ds(pl.multiple_of(c * half + first, 16), count)
+
+    def z_copies(o, c, d):
+        there = (p + ways[d][1] + length) % length * 2 + side
+        tail = x_buf.at[o, side, at_rows(c, 0, keep)]
+        copies = [copy_to("sp", there, tail, tail, zt_s.at[c, o, d], zt_r.at[c, o, d])]
+        if cross:
+            head = x_buf.at[o, :, at_rows(c, keep, cross)]
+            copies.append(copy_to("sp", there, head, head, zh_s.at[c, o, d], zh_r.at[c, o, d]))
+        return copies
+
+    def y_copy(o, c):
+        tail = x_buf.at[o, side, at_rows(c, 0, keep)]
+        return copy_to("sp", mate, tail, tail, yt_s.at[c, o], yt_r.at[c, o])
+
+    def swap_copy(c):
+        head = x_buf.at[p, side, at_rows(c, keep, cross)]
+        return copy_to("sp", mate, head, head, yh_s.at[c], yh_r.at[c])
+
+    def hidden_copy(o, c):
+        r = at_rows(c, 0, half)
+        return copy_to(
+            "sp", mate, hid_out.at[o, r], hid.at[o, r, pl.ds(hidden, hidden)], h_s.at[c, o], h_r.at[c, o]
+        )
+
+    def sum_copy(t, c, d):
+        r = at_rows(c, 0, half)
+        there = (p + ways[d][1] + length) % length * 2 + side
+        return copy_to(
+            "sp", there, red_out.at[t, r], red_in.at[t, d, r], red_s.at[c, t], red_r.at[c, t, d]
+        )
+
+    def behind(d):
+        return p if d == 0 else last - p
+
+    def arrival(d, j):
+        count = behind(d)
+        c = jnp.where(j > count, 1, 0)
+        far = jnp.where(j > count, 2 * count + 1 - j, j)
+        o = jnp.clip(p - ways[d][1] * far, 0, last)
+        return jnp.logical_and(j >= 1, j <= 2 * count), o, c
+
+    def ahead(d):
+        return on_line(p + ways[d][1], length)
+
+    def send_on(o, c, d):
+        @pl.when(ahead(d))
+        def _():
+            for copy in z_copies(o, c, d):
+                copy.start()
+
+    def gate_up(o, c):
+        r = at_rows(c, 0, half)
+        weight = w_col[pl.ds(o * 2, 2), r, :].reshape(2 * half, lanes)
+
+        def tile(j, carry):
+            rows_in = x_buf[o, :, r, :].reshape(2 * half, width)
+            both = jnp.dot(rows_in, w_in[:, pl.ds(pl.multiple_of(j * 2 * lanes, 2 * lanes), 2 * lanes)],
+                           preferred_element_type=f32)
+            gate_act = jnp.minimum(both[:, :lanes], 7.0)
+            up_act = jnp.clip(both[:, lanes:], -7.0, 7.0)
+            value = gate_act * jax.nn.sigmoid(1.702 * gate_act) * (up_act + 1.0) * weight
+            mine = side == 0
+            col = pl.ds(pl.multiple_of(j * lanes, lanes), lanes)
+            hid[o, r, col] = jnp.where(mine, value[:half], value[half:]).astype(bf16)
+            hid_out[o, r, col] = jnp.where(mine, value[half:], value[:half]).astype(bf16)
+            return carry
+
+        lax.fori_loop(0, tiles, tile, 0)
+        hidden_copy(o, c).start()
+
+    def down_rows(o, c):
+        hidden_copy(o, c).wait_recv()
+        r = at_rows(c, 0, half)
+        step = 2 * lanes
+
+        def tile(j, carry):
+            col = pl.ds(pl.multiple_of(j * step, step), step)
+            part[o, r, col] = jnp.dot(hid[o, r, :], w_out[:, col], preferred_element_type=f32)
+            return carry
+
+        lax.fori_loop(0, width // step, tile, 0)
+
+    def flow(t, c, d, valid):
+        r = at_rows(c, 0, half)
+        t = jnp.clip(t, 0, last)
+        final = t == p
+        incoming = on_line(p - ways[d][1], length)
+
+        @pl.when(jnp.logical_and(valid, incoming))
+        def _():
+            sum_copy(t, c, d).wait_recv()
+            part[t, r, :] += red_in[t, d, r, :].astype(f32)
+
+        @pl.when(jnp.logical_and(valid, jnp.logical_not(final)))
+        def _():
+            red_out[t, r, :] = part[t, r, :].astype(bf16)
+            sum_copy(t, c, d).start()
+
+    place_own.wait()
+    for c in range(2):
+        if cross:
+            swap_copy(c).start()
+    for d in range(2):
+        @pl.when(ahead(d))
+        def _():
+            z_copies(p, 0, d)[0].start()
+    y_copy(p, 0).start()
+    down_y.start()
+    for step in range(1, n):
+        weight_copy(step).start()
+    w_row[me] = spread[me]
+    if cross:
+        swap_copy(0).wait_recv()
+    for d in range(2):
+        @pl.when(ahead(d))
+        def _():
+            for copy in z_copies(p, 0, d)[1:]:
+                copy.start()
+    for step in range(1, n):
+        weight_copy(step).wait_recv()
+    for k in range(n):
+        w_col[k] = jnp.broadcast_to(w_row[k, 0, :][None, :], (lanes, rows)).T
+    for load in loads:
+        load.wait()
+    if cross:
+        swap_copy(1).wait_recv()
+    for d in range(2):
+        @pl.when(behind(d) == 0)
+        def _():
+            send_on(p, 1, d)
+    down_y.wait_recv()
+    for step in range(1, t_n // 2):
+        down_x(step).start()
+    for step in range(t_n // 2):
+        if step:
+            down_x(step).wait_recv()
+        down_mate(step).start()
+    for step in range(t_n // 2):
+        down_mate(step).wait_recv()
+
+    own_slot = length + 1
+
+    def slot(i, carry):
+        for d in range(2):
+            there, o, c = arrival(d, i + 1)
+
+            @pl.when(there)
+            def _():
+                for copy in z_copies(o, c, d):
+                    copy.wait_recv()
+                send_on(o, c, d)
+                y_copy(o, c).start()
+
+            @pl.when(jnp.logical_and(i + 1 == 2 * behind(d), behind(d) > 0))
+            def _():
+                send_on(p, 1, d)
+
+        @pl.when(i + 1 == own_slot)
+        def _():
+            y_copy(p, 1).start()
+
+        for d in range(2):
+            there, o, c = arrival(d, i)
+
+            @pl.when(there)
+            def _():
+                y_copy(o, c).wait_recv()
+                gate_up(o, c)
+
+        own_now = jnp.logical_or(i == 0, i == own_slot)
+        own_c = jnp.where(i == 0, 0, 1)
+
+        @pl.when(own_now)
+        def _():
+            y_copy(p, own_c).wait_recv()
+            gate_up(p, own_c)
+
+        for d in range(2):
+            there, o, c = arrival(d, i - 1)
+
+            @pl.when(there)
+            def _():
+                down_rows(o, c)
+
+        own_then = jnp.logical_or(i == 1, i == own_slot + 1)
+        then_c = jnp.where(i == 1, 0, 1)
+
+        @pl.when(own_then)
+        def _():
+            down_rows(p, then_c)
+
+        f = i - 1
+        for d in range(2):
+            q = behind(d)
+            for c in range(2):
+                reach = f - q if c == 0 else 2 * length - 1 - f + q
+                valid = jnp.logical_and(jnp.logical_and(reach >= q, reach <= last), f >= 0)
+                t = reach if d == 0 else last - reach
+                flow(t, c, d, valid)
+        return carry
+
+    lax.fori_loop(0, 2 * length + 1, slot, 0)
+    out[...] = part[p]
+
+    down_y.wait_send()
+    for step in range(t_n // 2):
+        if step:
+            down_x(step).wait_send()
+        down_mate(step).wait_send()
+    for step in range(1, n):
+        weight_copy(step).wait_send()
+    for c in range(2):
+        if cross:
+            swap_copy(c).wait_send()
+        for o in range(length):
+            y_copy(o, c).wait_send()
+            hidden_copy(o, c).wait_send()
+
+            @pl.when(o != p)
+            def _():
+                sum_copy(o, c, 0).wait_send()
+
+            for d in range(2):
+                passes = o <= p if d == 0 else o >= p
+
+                @pl.when(jnp.logical_and(passes, ahead(d)))
+                def _():
+                    for copy in z_copies(o, c, d):
+                        copy.wait_send()
+
+
+def fits_line(normed, gate_w):
+    n, t_n = lax.axis_size("sp"), lax.axis_size("tp")
+    rows, width = normed.shape
+    hidden = gate_w.shape[2]
+    return (n % 2 == 0 and t_n % 2 == 0 and rows % 128 == 0 and rows == 128
+            and width % 256 == 0 and hidden % 128 == 0 and hidden % (16 * t_n) == 0)
+
+
+def expert_layer(normed, routes, route_weight, gate_w, up_w, down_w):
+    n, t_n = lax.axis_size("sp"), lax.axis_size("tp")
+    rows, width = normed.shape
+    hidden = gate_w.shape[2]
+    length = n // 2
+    named = routes[:, :, None] == jnp.arange(n, dtype=jnp.int32)[None, None, :]
+    spread = jnp.sum(jnp.where(named, route_weight[:, :, None], 0.0), axis=1).T[:, None, :]
+    vmem = pl.BlockSpec(memory_space=pltpu.VMEM)
+    hbm = pl.BlockSpec(memory_space=pl.ANY)
+    dma = pltpu.SemaphoreType.DMA
+    bf16 = jnp.bfloat16
+    return pl.pallas_call(
+        functools.partial(expert_kernel, n, t_n, 16),
+        out_shape=jax.ShapeDtypeStruct((rows, width), jnp.float32),
+        in_specs=[vmem, vmem, hbm, hbm, hbm],
+        out_specs=vmem,
+        scratch_shapes=[
+            pltpu.VMEM((length, 2, rows, width), bf16),
+            pltpu.VMEM((width, 2 * hidden), bf16),
+            pltpu.VMEM((2 * hidden, width), bf16),
+            pltpu.VMEM((length, rows, 2 * hidden), bf16),
+            pltpu.VMEM((length, rows, hidden), bf16),
+            pltpu.VMEM((length, rows, width), jnp.float32),
+            pltpu.VMEM((length, 2, rows, width), bf16),
+            pltpu.VMEM((length, rows, width), bf16),
+            pltpu.VMEM((n, 1, rows), jnp.float32),
+            pltpu.VMEM((n, rows, 128), jnp.float32),
+            dma((2 * (hidden // 128) + 2,)),
+            dma((n,)), dma((n,)),
+            dma((2, length, 2)), dma((2, length, 2)),
+            dma((2, length, 2)), dma((2, length, 2)),
+            dma((2, length)), dma((2, length)),
+            dma((2,)), dma((2,)),
+            dma((2, length)), dma((2, length)),
+            dma((2, length)), dma((2, length, 2)),
+            dma, dma,
+            dma((t_n,)), dma((t_n,)),
+            dma((t_n,)), dma((t_n,)),
+        ],
+        compiler_params=pltpu.CompilerParams(collective_id=1, has_side_effects=True),
+    )(normed, spread, gate_w, up_w, down_w)
 
 
 def body(
@@ -431,7 +778,10 @@
         projected = lax.psum_scatter(share, "tp", scatter_dimension=0, tiled=True)
     stream = (resid.astype(jnp.float32) + rms_norm(projected, post_gain)).astype(jnp.bfloat16)
     normed = rms_norm(stream.astype(jnp.float32), pre_gain).astype(jnp.bfloat16)
-    mix = every_row if whole_rows else by_slot
+    if whole_rows:
+        mix = expert_layer if fits_line(normed, gate_w) else every_row
+    else:
+        mix = by_slot
     combined = mix(normed, routes, route_weight, gate_w, up_w, down_w)
     return (stream.astype(jnp.float32) + rms_norm(combined, moe_gain)).astype(jnp.bfloat16)
 

time: 168 us -> 154 us (0.917)
  the two profiles are of different devices: /device:TPU:8 before, /device:TPU:15 now
where the time goes in v1:
time: 154 us; the launch traced here: 153 us
  Pallas kernels  137 us (89%)
  other arithmetic  9.7 us (6%)
  starting transfers between devices  3.15 us (2%)
  matrix products  2.79 us (2%)
    pallas_call x1, Pallas kernels, expert_layer(): pl.pallas_call(functools.partial(expert_kernel, n, t_n, 16), out_shape=ja...  117 us
    pallas_call x1, Pallas kernels, reduce_rows(): pl.pallas_call(functools.partial(reduce_kernel, axis, n, early), out_shap...  20.4 us
    reduce_sum x3, other arithmetic, rms_norm(): jnp.mean(vector * vector, axis=-1, keepdims=True) + epsilon  4.36 us
    ppermute x1, starting transfers between devices, shifted(): return lax.ppermute(shard, axis, pairs)  3.15 us
  transfers between devices with their start and end apart: 1, of which 1 were waited for; matrix products, arithmetic and copies ran while one was open for 0% of the time, Pallas kernels for 0%

profile of v1, /device:TPU:15, one launch (start us, length us, event | category | flops | bytes accessed | tf_op | source)
XLA Modules:
  0.0 153.3 jit_solution(11079913483759795201)
XLA Ops:
  0.0 0.0 copy-start
  0.0 0.0 copy-start.5
  0.0 0.0 copy-start.7
  0.0 0.0 copy-start.6
  0.0 0.0 copy-start.8
  0.0 1.5 convert_multiply_fusion.2
  1.5 3.1 %collective-permute-start = (f32[2,512]{1,0:T(2,128)S(1)}, f32[2,512]{1,0:T(2,128)S(1)}, u32[]{:S(2)}, u32[]{:S(2)}) collective-permute-start(f32[2,512]{1,0:T(2,128)S(1)} %slice.24), channel_id=1, source_target_pairs={{0,4},{4,8},{8,12},{12,16},{16,20},{20,24},{24,28},{1,5},{5,9},{9,... | collective-permute-start | bytes 12296 | tf_op jit(solution)/shard_map/ppermute | solution.py:16
  4.7 0.0 copy-done.5
  4.7 0.0 copy-done.7
  4.7 0.0 copy-done.6
  4.7 0.6 select_reduce_fusion
  5.3 0.6 collective-permute-done
  5.9 0.0 copy-done
  5.9 0.0 copy-done.8
  5.9 2.8 %convolution_convert_fusion = bf16[512,2048]{1,0:T(8,128)(2,1)} fusion(bf16[512,2048]{1,0:T(8,128)(2,1)S(1)} %copy-done, f32[2,512]{1,0:T(2,128)S(1)} %collective-permute-done, f32[512,512]{1,0:T(8,128)S(1)} %convert_multiply_fusion.2, bf16[512,512]{1,0:T(8,128)(2,1)S(1)} %copy-done.8, f32[512]{0:T(512)S(1)} %bitcast.11, f32[512]{0:T(512)S(1)} %bitcast.12, ...), kind=kOutput, calls=%fused_computation | convolution fusion | flops 1077411840 | bytes 5777408 | tf_op jit(solution)/shard_map/dot_general | solution.py:773
  8.7 0.0 copy-start.1
  8.7 0.0 copy-start.2
  8.7 20.4 %shard_map.136 = f32[128,2048]{1,0:T(8,128)} custom-call(bf16[4,128,2048]{2,1,0:T(8,128)(2,1)} %bitcast.8), custom_call_target="tpu_custom_call" | custom-call | tf_op jit(solution)/shard_map/pallas_call | solution.py:358
  29.1 0.0 copy-start.3
  29.1 1.4 multiply_reduce_fusion.1
  30.5 0.0 copy-done.1
  30.5 0.0 copy-done.2
  30.5 1.6 %fusion.6 = (f32[128]{0:T(128)S(1)}, bf16[128,2048]{1,0:T(8,128)(2,1)S(1)}) fusion(f32[2048]{0:T(1024)S(1)} %copy-done.2, f32[128,2048]{1,0:T(8,128)} %shard_map.136, f32[128]{0:T(128)S(1)} %add_rsqrt_fusion.2, bf16[128,2048]{1,0:T(8,128)(2,1)S(1)} %copy-done.1), kind=kLoop, calls=%fused_computation.12 | loop fusion | flops 2097024 | bytes 2106368 | tf_op jit(solution)/shard_map/reduce_sum | solution.py:20
  32.1 0.0 copy-done.3
  32.2 1.0 fusion.8.own
  33.1 0.0 copy-start.4
  33.1 116.5 %shard_map.137 = f32[128,2048]{1,0:T(8,128)} custom-call(bf16[128,2048]{1,0:T(8,128)(2,1)} %fusion.8.own, f32[8,1,128]{2,1,0:T(1,128)} %bitcast.9, bf16[1,2048,640]{2,1,0:T(8,128)(2,1)} %gate.1, bf16[1,2048,640]{2,1,0:T(8,128)(2,1)} %up.1, bf16[1,640,2048]{2,1,0:T(8,128)(2,1)} %down.1), custom_call_target="tpu_custom_call" | custom-call | tf_op jit(solution)/shard_map/pallas_call | solution.py:712
  149.7 1.4 multiply_reduce_fusion
  151.1 0.0 copy-done.4
  151.1 2.2 %fusion.9 = bf16[128,2048]{1,0:T(8,128)(2,1)} fusion(bf16[128,2048]{1,0:T(8,128)(2,1)S(1)} %get-tuple-element.6, f32[128,2048]{1,0:T(8,128)} %shard_map.137, f32[2048]{0:T(1024)S(1)} %copy-done.4, f32[128]{0:T(128)S(1)} %add_rsqrt_fusion), kind=kLoop, calls=%fused_computation.15 | loop fusion | flops 1310720 | bytes 2105856 | tf_op jit(solution)/shard_map/convert_element_type | solution.py:786
  (5 shorter events, 0.0 us)
Async XLA Ops:
  0.0 5.9 %copy-start = (bf16[512,2048]{1,0:T(8,128)(2,1)S(1)}, bf16[512,2048]{1,0:T(8,128)(2,1)}, u32[]{:S(2)}) copy-start(bf16[512,2048]{1,0:T(8,128)(2,1)} %param.18) | copy-start | bytes 6291460
  0.0 4.7 %copy-start.5 = (f32[3,512]{1,0:T(4,128)S(1)}, f32[3,512]{1,0:T(4,128)}, u32[]{:S(2)}) copy-start(f32[3,512]{1,0:T(4,128)} %param.17) | copy-start | bytes 18436
  0.0 4.7 %copy-start.7 = (s32[128,4]{0,1:T(4,128)S(1)}, s32[128,4]{0,1:T(4,128)}, u32[]{:S(2)}) copy-start(s32[128,4]{0,1:T(4,128)} %param.23) | copy-start | bytes 6148
  0.0 4.7 %copy-start.6 = (f32[128,4]{0,1:T(4,128)S(1)}, f32[128,4]{0,1:T(4,128)}, u32[]{:S(2)}) copy-start(f32[128,4]{0,1:T(4,128)} %param.24) | copy-start | bytes 6148
  0.0 5.9 %copy-start.8 = (bf16[512,512]{1,0:T(8,128)(2,1)S(1)}, bf16[512,512]{1,0:T(8,128)(2,1)}, u32[]{:S(2)}) copy-start(bf16[512,512]{1,0:T(8,128)(2,1)} %param.14) | copy-start | bytes 1572868
  1.5 4.4 %collective-permute-start = (f32[2,512]{1,0:T(2,128)S(1)}, f32[2,512]{1,0:T(2,128)S(1)}, u32[]{:S(2)}, u32[]{:S(2)}) collective-permute-start(f32[2,512]{1,0:T(2,128)S(1)} %slice.24), channel_id=1, source_target_pairs={{0,4},{4,8},{8,12},{12,16},{16,20},{20,24},{24,28},{1,5},{5,9},{9,... | collective-permute-start | bytes 12296 | tf_op jit(solution)/shard_map/ppermute | solution.py:16
  8.7 21.8 %copy-start.1 = (bf16[128,2048]{1,0:T(8,128)(2,1)S(1)}, bf16[128,2048]{1,0:T(8,128)(2,1)}, u32[]{:S(2)}) copy-start(bf16[128,2048]{1,0:T(8,128)(2,1)} %param.19) | copy-start | bytes 1572868
  8.7 21.8 %copy-start.2 = (f32[2048]{0:T(1024)S(1)}, f32[2048]{0:T(1024)}, u32[]{:S(2)}) copy-start(f32[2048]{0:T(1024)} %param.20) | copy-start | bytes 24580
  29.1 3.0 %copy-start.3 = (f32[2048]{0:T(1024)S(1)}, f32[2048]{0:T(1024)}, u32[]{:S(2)}) copy-start(f32[2048]{0:T(1024)} %param.21) | copy-start | bytes 24580
  33.1 117.9 %copy-start.4 = (f32[2048]{0:T(1024)S(1)}, f32[2048]{0:T(1024)}, u32[]{:S(2)}) copy-start(f32[2048]{0:T(1024)} %param.22) | copy-start | bytes 24580
